TPU v7x, 32 devices: a whole 2x2x4 slice. The times are simulated.
32 devices in a mesh: sp: 4 (over y, x), tp: 8 (over z, core).
Axes of the slice: x: 2, y: 2, z: 4, core: 2. Of those that a mesh axis runs over, the one named last changes fastest.
Arguments:
- latent: bfloat16 [4096, 2048], P(('sp', 'tp')), may hold values from -1.5 to 1.5
- context: bfloat16 [128, 2048], P('sp'), may hold values from -6 to 6
- cond: bfloat16 [2048], replicated, may hold values from -6 to 6
- cond_context: bfloat16 [2048], replicated, may hold values from -6 to 6
- mod_weight: bfloat16 [3, 2048, 2048], P(None, 'sp', 'tp'), may hold values from -0.125 to 0.125
- norm_gain: bfloat16 [2048], replicated, may hold values from 0.099609375 to 1.8984375
- down_q: bfloat16 [2048, 768], P('tp'), may hold values from -0.125 to 0.125
- down_kv: bfloat16 [2048, 512], P('tp'), may hold values from -0.125 to 0.125
- rope_weight: bfloat16 [2048, 32], replicated, may hold values from -0.125 to 0.125
- qlat_gain: bfloat16 [768], replicated, may hold values from 0.099609375 to 1.8984375
- kvlat_gain: bfloat16 [512], replicated, may hold values from 0.099609375 to 1.8984375
- up_query: bfloat16 [768, 1536], P(None, 'tp'), may hold values from -0.21875 to 0.21875
- up_key: bfloat16 [512, 1024], P(None, 'tp'), may hold values from -0.25 to 0.25
- up_value: bfloat16 [512, 1024], P(None, 'tp'), may hold values from -0.25 to 0.25
- query_gain: float32 [96], replicated, may hold values from 0.5 to 8
- key_gain: float32 [96], replicated, may hold values from 0.5 to 8
- context_bias: float32 [16], P('tp'), may hold values from -2.2 to -0.7
- out_weight: bfloat16 [1024, 2048], P('tp'), may hold values from -24 to 24
Outputs:
- mixed: bfloat16 [4096, 2048], P(('sp', 'tp'))
All inputs are finite; a program needn't handle non-finite values.
Results may differ from a plain program's by a relative error of at most 0.028.
The roundings to bfloat16 on the way count: a program that leaves them out, or rounds other values in their place, can miss the bound.
Values may be sent and summed in bfloat16 or wider, within the bound.
A program may use at most 64 MiB of HBM per device.

v0:
```python
import math
import jax
import jax.numpy as jnp
from jax import lax
from jax.sharding import PartitionSpec as P

NOPE = 64
ROPE = 32
VDIM = 64
GRID_W = 64
TOK_DEV = 1024
CTX_DEV = 32
epsilon = 1e-06
theta = 10000.0


def rms_scale(tensor, gain):
    return (
        tensor
        * lax.rsqrt(jnp.mean(tensor * tensor, axis=-1, keepdims=True) + epsilon)
        * gain.astype(jnp.float32)
    )


def axial_tables(positions):
    pair_count = ROPE // 4
    frequency = jnp.power(theta, -jnp.arange(pair_count, dtype=jnp.float32) / pair_count)
    row_angle = (positions // GRID_W).astype(jnp.float32)[:, None] * frequency
    col_angle = (positions % GRID_W).astype(jnp.float32)[:, None] * frequency
    return (jnp.cos(row_angle), jnp.sin(row_angle), jnp.cos(col_angle), jnp.sin(col_angle))


def rotate_half(tensor, cosine, sine_table):
    first, second = jnp.split(tensor, 2, axis=-1)
    cosine = cosine[:, None, :]
    sine_table = sine_table[:, None, :]
    return jnp.concatenate(
        [first * cosine - second * sine_table, second * cosine + first * sine_table], axis=-1
    )


def axial_rotate(tensor, tables):
    half_width = tensor.shape[-1] // 2
    return jnp.concatenate(
        [
            rotate_half(tensor[..., :half_width], tables[0], tables[1]),
            rotate_half(tensor[..., half_width:], tables[2], tables[3]),
        ],
        axis=-1,
    )


def modulate(row_block, gain, shifts, scales):
    normal = rms_scale(row_block.astype(jnp.float32), gain)
    return (normal * (1.0 + scales) + shifts).astype(jnp.bfloat16)


def make_queries(query_latent, up_query, query_gain, tables):
    amount = query_latent.shape[0]
    projected = jnp.dot(query_latent, up_query, preferred_element_type=jnp.float32).reshape(
        amount, -1, NOPE + ROPE
    )
    normal = rms_scale(projected, query_gain)
    return jnp.concatenate(
        [normal[..., :NOPE], axial_rotate(normal[..., NOPE:], tables)], axis=-1
    ).astype(jnp.bfloat16)


def make_keys(kv_latent, rope_rows, up_key, up_value, key_gain, tables):
    amount = kv_latent.shape[0]
    unrotated = jnp.dot(kv_latent, up_key, preferred_element_type=jnp.float32).reshape(
        amount, -1, NOPE
    )
    head_count = unrotated.shape[1]
    shared = jnp.broadcast_to(rope_rows.astype(jnp.float32)[:, None, :], (amount, head_count, ROPE))
    normal = rms_scale(jnp.concatenate([unrotated, shared], axis=-1), key_gain)
    if tables is not None:
        normal = jnp.concatenate(
            [normal[..., :NOPE], axial_rotate(normal[..., NOPE:], tables)], axis=-1
        )
    values = jnp.dot(kv_latent, up_value, preferred_element_type=jnp.float32).reshape(
        amount, head_count, VDIM
    )
    return (normal.astype(jnp.bfloat16), values.astype(jnp.bfloat16))


def absorb_block(state_in, queries, key_block, value_block, shift_heads):
    run_max, run_sum, run_acc = state_in
    scores = jnp.einsum("qhd,khd->qhk", queries, key_block, preferred_element_type=jnp.float32) * (
        NOPE + ROPE
    ) ** (-0.5)
    scores = scores + shift_heads[None, :, None]
    new_max = jnp.maximum(run_max, jnp.max(scores, axis=-1))
    factor = jnp.exp(run_max - new_max)
    weights = jnp.exp(scores - new_max[..., None])
    run_sum = run_sum * factor + jnp.sum(weights, axis=-1)
    run_acc = run_acc * factor[..., None] + jnp.einsum(
        "qhk,khd->qhd",
        weights.astype(jnp.bfloat16),
        value_block,
        preferred_element_type=jnp.float32,
    )
    return (new_max, run_sum, run_acc)


def shards(
    latent,
    context,
    cond,
    cond_context,
    mod_weight,
    norm_gain,
    down_q,
    down_kv,
    rope_weight,
    qlat_gain,
    kvlat_gain,
    up_query,
    up_key,
    up_value,
    query_gain,
    key_gain,
    context_bias,
    out_weight,
):
    seq_index = lax.axis_index("sp")
    tp_count = lax.axis_size("tp")
    own_rows = latent.shape[0]
    block_tokens = own_rows * tp_count
    row_span = mod_weight.shape[1]
    activated = jax.nn.silu(jnp.stack([cond, cond_context]).astype(jnp.float32)).astype(
        jnp.bfloat16
    )
    own_part = lax.dynamic_slice_in_dim(activated, seq_index * row_span, row_span, 1)
    partial_value = jnp.concatenate(
        [
            jnp.einsum("d,rde->re", own_part[0], mod_weight, preferred_element_type=jnp.float32),
            jnp.einsum(
                "d,rde->re", own_part[1], mod_weight[:2], preferred_element_type=jnp.float32
            ),
        ],
        axis=0,
    )
    summed = lax.psum(partial_value, "sp")
    modulations = lax.all_gather(summed, "tp", axis=1, tiled=True)
    normed = modulate(latent, norm_gain, modulations[0], modulations[1])
    context_normed = modulate(context, norm_gain, modulations[3], modulations[4])
    stacked = jnp.concatenate([normed, context_normed], axis=0)
    pieces = (
        lax.all_gather(down_q, "tp", axis=0, tiled=True),
        lax.all_gather(down_kv, "tp", axis=0, tiled=True),
    )
    columns = stacked
    query_down = jnp.dot(columns[:own_rows], pieces[0], preferred_element_type=jnp.float32)
    kv_down = jnp.dot(columns, pieces[1], preferred_element_type=jnp.float32)
    query_latent = rms_scale(query_down, qlat_gain).astype(jnp.bfloat16)
    kv_latent = rms_scale(kv_down, kvlat_gain).astype(jnp.bfloat16)
    rope_rows = jnp.dot(stacked, rope_weight, preferred_element_type=jnp.float32).astype(
        jnp.bfloat16
    )
    all_query, all_kv, all_rope = (
        lax.all_gather(query_latent, "tp", axis=0, tiled=True),
        lax.all_gather(kv_latent[:own_rows], "tp", axis=0, tiled=True),
        lax.all_gather(rope_rows[:own_rows], "tp", axis=0, tiled=True),
    )
    own_context_keys, own_context_values = make_keys(
        kv_latent[own_rows:], rope_rows[own_rows:], up_key, up_value, key_gain, None
    )
    context_keys, context_values = (
        lax.all_gather(own_context_keys, "sp", axis=0, tiled=True),
        lax.all_gather(own_context_values, "sp", axis=0, tiled=True),
    )
    positions = seq_index * block_tokens + jnp.arange(block_tokens, dtype=jnp.int32)
    tables = axial_tables(positions)
    queries = make_queries(all_query, up_query, query_gain, tables)
    keys, values = make_keys(all_kv, all_rope, up_key, up_value, key_gain, tables)
    head_count = queries.shape[1]
    shift_heads = context_bias + math.log(TOK_DEV / CTX_DEV)
    start_state = (
        jnp.full((block_tokens, head_count), -jnp.inf, jnp.float32),
        jnp.zeros((block_tokens, head_count), jnp.float32),
        jnp.zeros((block_tokens, head_count, VDIM), jnp.float32),
    )
    state_now = absorb_block(start_state, queries, context_keys, context_values, shift_heads)
    no_shift = jnp.zeros((head_count,), jnp.float32)
    pieces = (
        lax.all_gather(keys, "sp", axis=0, tiled=True),
        lax.all_gather(values, "sp", axis=0, tiled=True),
    )
    amount = pieces[0].shape[0]
    span_rows = math.gcd(amount, 1024)
    key_blocks = pieces[0].reshape(amount // span_rows, span_rows, head_count, pieces[0].shape[2])
    value_blocks = pieces[1].reshape(amount // span_rows, span_rows, head_count, pieces[1].shape[2])

    def scan_step(state_mid, blocks):
        return (absorb_block(state_mid, queries, blocks[0], blocks[1], no_shift), None)

    state_out, unused = lax.scan(scan_step, state_now, (key_blocks, value_blocks))
    run_max, run_sum, run_acc = state_out
    attended = (
        (run_acc / run_sum[..., None]).astype(jnp.bfloat16).reshape(block_tokens, head_count * VDIM)
    )
    token_rows = lax.all_to_all(attended, "tp", split_axis=0, concat_axis=1, tiled=True)
    columns = token_rows
    projected = jnp.dot(
        columns,
        lax.all_gather(out_weight, "tp", axis=0, tiled=True),
        preferred_element_type=jnp.float32,
    )
    return (latent.astype(jnp.float32) + modulations[2] * projected).astype(jnp.bfloat16)


def solution(mesh):
    in_specs = (
        P(("sp", "tp"), None),
        P("sp", None),
        P(),
        P(),
        P(None, "sp", "tp"),
        P(),
        P("tp", None),
        P("tp", None),
        P(),
        P(),
        P(),
        P(None, "tp"),
        P(None, "tp"),
        P(None, "tp"),
        P(),
        P(),
        P("tp"),
        P("tp", None),
    )
    out_specs = P(("sp", "tp"), None)
    return jax.shard_map(shards, mesh=mesh, in_specs=in_specs, out_specs=out_specs, check_vma=False)
```

profile of v0, /device:TPU:0, one launch (start us, length us, event | category | flops | bytes accessed | tf_op | source)
XLA Modules:
  0.0 254.6 jit_solution(11585700958939711861)
XLA Ops:
  9.5 1.3 fusion.62
  13.5 11.5 %psum.7 = f32[5,256]{1,0:T(8,128)S(1)} all-reduce(f32[5,256]{1,0:T(8,128)S(1)} %pad_maximum_fusion.5), channel_id=1, replica_groups=mesh['sp'=4,'tp'=8] {'sp'}, use_global_device_ids=true, to_apply=%region_0.1 | all-reduce | flops 1280 | bytes 10240 | tf_op jit(solution)/shard_map/psum | solution.py:144
  25.0 14.7 %all_gather.33 = f32[5,2048]{1,0:T(8,128)S(1)} all-gather(f32[5,256]{1,0:T(8,128)S(1)} %psum.7), channel_id=1, replica_groups=mesh['sp'=4,'tp'=8] {'tp'}, dimensions={1}, use_global_device_ids=true | all-gather | bytes 46080 | tf_op jit(solution)/shard_map/all_gather | solution.py:145
  44.4 2.2 multiply_reduce_fusion.3
  47.6 33.1 %all-gather.10.cloned.1.call-done = bf16[2048,768]{1,0:T(8,128)(2,1)} async-done(((bf16[256,768]{1,0:T(8,128)(2,1)}), bf16[2048,768]{1,0:T(8,128)(2,1)}) %all-gather.10.cloned.1.call-update) | async-done | bytes 3145744 | tf_op jit(solution)/shard_map/all_gather | solution.py:150
  80.7 2.6 %multiply_reduce_fusion.2 = (f32[128]{0:T(128)S(1)}, f32[128,768]{1,0:T(8,128)S(1)}) fusion(bf16[128,2048]{1,0:T(8,128)(2,1)S(1)} %fusion.28, bf16[2048,768]{1,0:T(8,128)(2,1)} %all-gather.10.cloned.1.call-done), kind=kOutput, calls=%fused_computation.55 | convolution fusion | flops 402849664 | bytes 4063744 | tf_op jit(solution)/shard_map/dot_general | solution.py:154
  84.4 13.1 %all_gather.40 = bf16[1024,32]{0,1:T(8,128)(2,1)S(1)} all-gather(bf16[128,32]{0,1:T(8,128)(2,1)S(1)} %slice.87), channel_id=1, replica_groups=mesh['sp'=4,'tp'=8] {'tp'}, dimensions={0}, use_global_device_ids=true | all-gather | bytes 73728 | tf_op jit(solution)/shard_map/all_gather | solution.py:164
  97.9 5.5 %all-gather.14.cloned.1.call-done = bf16[1024,512]{1,0:T(8,128)(2,1)} async-done(((bf16[128,512]{1,0:T(8,128)(2,1)}), bf16[1024,512]{1,0:T(8,128)(2,1)}) %all-gather.14.cloned.1.call-update) | async-done | bytes 1048592 | tf_op jit(solution)/shard_map/all_gather | solution.py:163
  103.4 1.8 fusion.69
  106.8 23.0 %all-gather.12.cloned.1.call-done = bf16[1024,768]{1,0:T(8,128)(2,1)} async-done(((bf16[128,768]{1,0:T(8,128)(2,1)}), bf16[1024,768]{1,0:T(8,128)(2,1)}) %all-gather.12.cloned.1.call-update) | async-done | bytes 1572880 | tf_op jit(solution)/shard_map/all_gather | solution.py:162
  129.8 2.1 fusion.68
  134.6 8.7 %all_gather.35 = bf16[128,2,96]{2,0,1:T(8,128)(2,1)S(1)} all-gather(bf16[32,2,96]{2,0,1:T(8,128)(2,1)S(1)} %multiply_convert_fusion.2), channel_id=1, replica_groups=mesh['sp'=4,'tp'=8] {'sp'}, dimensions={0}, use_global_device_ids=true | all-gather | bytes 61440 | tf_op jit(solution)/shard_map/all_gather | solution.py:170
  143.3 8.2 %all_gather.38 = bf16[128,2,64]{2,0,1:T(8,128)(2,1)S(1)} all-gather(bf16[32,2,64]{2,0,1:T(8,128)(2,1)S(1)} %copy.43), channel_id=1, replica_groups=mesh['sp'=4,'tp'=8] {'sp'}, dimensions={0}, use_global_device_ids=true | all-gather | bytes 40960 | tf_op jit(solution)/shard_map/all_gather | solution.py:171
  151.6 5.9 %all-gather.18.cloned.1.call-done = bf16[4096,2,64]{0,2,1:T(8,128)(2,1)} async-done(((bf16[1024,2,64]{0,2,1:T(8,128)(2,1)}), bf16[4096,2,64]{0,2,1:T(8,128)(2,1)}) %all-gather.18.cloned.1.call-update) | async-done | bytes 1048592 | tf_op jit(solution)/shard_map/all_gather | solution.py:188
  157.4 2.3 copy.60
  160.5 29.4 %all-gather.16.cloned.1.call-done = bf16[4096,2,96]{0,2,1:T(8,128)(2,1)} async-done(((bf16[1024,2,96]{0,2,1:T(8,128)(2,1)}), bf16[4096,2,96]{0,2,1:T(8,128)(2,1)}) %all-gather.16.cloned.1.call-update) | async-done | bytes 1572880 | tf_op jit(solution)/shard_map/all_gather | solution.py:187
  189.9 1.6 copy.59
  191.5 21.5 %while.14 = (s32[]{:T(128)}, f32[1024,2]{0,1:T(2,128)S(1)}, f32[1024,2]{0,1:T(2,128)S(1)}, f32[1024,2,64]{0,2,1:T(8,128)S(1)}, bf16[4,1024,2,96]{1,3,2,0:T(8,128...) while((s32[]{:T(128)}, f32[1024,2]{0,1:T(2,128)S(1)}, ...), condition=%wide.region_13.14_spmd, body=%wide.region_10.13_spmd.sunk | while | flops 688132096 | bytes 27394648 | solution.py:198
  191.5 1.3 bitcast_reduce_fusion.2
  192.9 1.4 fusion.97
  194.3 2.6 %fusion.98 = f32[1024,2,64]{0,2,1:T(8,128)S(1)} fusion(f32[2,1024,1024]{2,1,0:T(8,128)S(1)} %get-tuple-element.168, f32[1024,2]{0,1:T(2,128)S(1)} %max.4, f32[1024,2,64]{0,2,1:T(8,128)S(1)} %get-tuple-element.182, bf16[4,1024,2,64]{1,3,2,0:T(8,128)(2,1)} %get-tuple-element.193, s32[]{:T(128)} %get-tuple-element.179, f32[1024,2]{0,1:T(2,128)S(1)} %get-tuple-element.170), kind=kOutput, calls=%fused_computation.7.clone.1 | convolution fusion | flops 274989056 | bytes 9716224 | tf_op jit(solution)/shard_map/while/body/eval_jaxpr/qhk,khd->qhd/dot_general | solution.py:97
  196.9 1.3 bitcast_reduce_fusion.2
  198.2 1.4 fusion.97
  199.6 2.6 %fusion.98 = f32[1024,2,64]{0,2,1:T(8,128)S(1)} fusion(f32[2,1024,1024]{2,1,0:T(8,128)S(1)} %get-tuple-element.168, f32[1024,2]{0,1:T(2,128)S(1)} %max.4, f32[1024,2,64]{0,2,1:T(8,128)S(1)} %get-tuple-element.182, bf16[4,1024,2,64]{1,3,2,0:T(8,128)(2,1)} %get-tuple-element.193, s32[]{:T(128)} %get-tuple-element.179, f32[1024,2]{0,1:T(2,128)S(1)} %get-tuple-element.170), kind=kOutput, calls=%fused_computation.7.clone.1 | convolution fusion | flops 274989056 | bytes 9716224 | tf_op jit(solution)/shard_map/while/body/eval_jaxpr/qhk,khd->qhd/dot_general | solution.py:97
  202.3 1.3 bitcast_reduce_fusion.2
  203.6 1.4 fusion.97
  205.0 2.6 %fusion.98 = f32[1024,2,64]{0,2,1:T(8,128)S(1)} fusion(f32[2,1024,1024]{2,1,0:T(8,128)S(1)} %get-tuple-element.168, f32[1024,2]{0,1:T(2,128)S(1)} %max.4, f32[1024,2,64]{0,2,1:T(8,128)S(1)} %get-tuple-element.182, bf16[4,1024,2,64]{1,3,2,0:T(8,128)(2,1)} %get-tuple-element.193, s32[]{:T(128)} %get-tuple-element.179, f32[1024,2]{0,1:T(2,128)S(1)} %get-tuple-element.170), kind=kOutput, calls=%fused_computation.7.clone.1 | convolution fusion | flops 274989056 | bytes 9716224 | tf_op jit(solution)/shard_map/while/body/eval_jaxpr/qhk,khd->qhd/dot_general | solution.py:97
  209.0 1.4 fusion.97
  210.4 2.6 %fusion.98 = f32[1024,2,64]{0,2,1:T(8,128)S(1)} fusion(f32[2,1024,1024]{2,1,0:T(8,128)S(1)} %get-tuple-element.168, f32[1024,2]{0,1:T(2,128)S(1)} %max.4, f32[1024,2,64]{0,2,1:T(8,128)S(1)} %get-tuple-element.182, bf16[4,1024,2,64]{1,3,2,0:T(8,128)(2,1)} %get-tuple-element.193, s32[]{:T(128)} %get-tuple-element.179, f32[1024,2]{0,1:T(2,128)S(1)} %get-tuple-element.170), kind=kOutput, calls=%fused_computation.7.clone.1 | convolution fusion | flops 274989056 | bytes 9716224 | tf_op jit(solution)/shard_map/while/body/eval_jaxpr/qhk,khd->qhd/dot_general | solution.py:97
  213.9 4.6 %all-to-all-start = ((bf16[8,128,128]{1,2,0:T(8,128)(2,1)}), bf16[8,128,128]{1,2,0:T(8,128)(2,1)S(1)}, u32[]{:S(2)}, u32[]{:S(2)}) async-start(bf16[8,128,128]{1,2,0:T(8,128)(2,1)} %copy.47), calls=%async_computation | async-start | bytes 524288 | tf_op jit(solution)/shard_map/all_to_all | solution.py:203
  218.5 25.6 %all-gather.20.cloned.1.call-done = bf16[1024,2048]{1,0:T(8,128)(2,1)} async-done(((bf16[128,2048]{1,0:T(8,128)(2,1)}), bf16[1024,2048]{1,0:T(8,128)(2,1)}) %all-gather.20.cloned.1.call-update) | async-done | bytes 4194320 | tf_op jit(solution)/shard_map/all_gather | solution.py:207
  244.1 3.7 %fusion.20 = bf16[128,2048]{1,0:T(8,128)(2,1)} fusion(bf16[128,1024]{0,1:T(8,128)(2,1)S(1)} %bitcast.112, bf16[1024,2048]{1,0:T(8,128)(2,1)} %all-gather.20.cloned.1.call-done, bf16[128,2048]{1,0:T(8,128)(2,1)S(1)} %copy-done.1, f32[2048]{0:T(1024)S(1)} %bitcast.113), kind=kOutput, calls=%fused_computation.20 | convolution fusion | flops 537919488 | bytes 5513216 | tf_op jit(solution)/shard_map/dot_general | solution.py:205
  (113 shorter events, 19.9 us)
Async XLA Ops:
  6.5 123.3 %copy-start = (bf16[768,192]{0,1:T(8,128)(2,1)S(1)}, bf16[768,192]{0,1:T(8,128)(2,1)}, u32[]{:S(2)}) copy-start(bf16[768,192]{0,1:T(8,128)(2,1)} %param.31) | copy-start | bytes 884740
  6.5 37.9 %all-gather.8.cloned.1.call-start = ((), (), s32[]{:S(2)}) async-start(), calls=%async_computation.1 | async-start | bytes 2359296 | tf_op jit(solution)/shard_map/all_gather | solution.py:151
  7.3 40.3 %copy-start.7 = (bf16[768]{0:T(1024)(128)(2,1)S(1)}, bf16[768]{0:T(1024)(128)(2,1)}, u32[]{:S(2)}) copy-start(bf16[768]{0:T(1024)(128)(2,1)} %param.29) | copy-start | bytes 4612
  7.3 73.4 %all-gather.10.cloned.1.call-start = ((), (), s32[]{:S(2)}) async-start(), calls=%async_computation.2 | async-start | bytes 3538944 | tf_op jit(solution)/shard_map/all_gather | solution.py:150
  8.0 95.4 %all-gather.14.cloned.1.call-start = ((), (), s32[]{:S(2)}) async-start(), calls=%async_computation.4 | async-start | bytes 1179648 | tf_op jit(solution)/shard_map/all_gather | solution.py:163
  44.4 39.7 %copy-start.9 = (bf16[2048,32]{0,1:T(8,128)(2,1)S(1)}, bf16[2048,32]{0,1:T(8,128)(2,1)}, u32[]{:S(2)}) copy-start(bf16[2048,32]{0,1:T(8,128)(2,1)} %param.28) | copy-start | bytes 393220
  46.7 56.7 %copy-start.4 = (bf16[512,128]{1,0:T(8,128)(2,1)S(1)}, bf16[512,128]{1,0:T(8,128)(2,1)}, u32[]{:S(2)}) copy-start(bf16[512,128]{1,0:T(8,128)(2,1)} %param.32) | copy-start | bytes 393220
  47.5 82.3 %all-gather.12.cloned.1.call-start = ((), (), s32[]{:S(2)}) async-start(), calls=%async_computation.3 | async-start | bytes 1769472 | tf_op jit(solution)/shard_map/all_gather | solution.py:162
  47.5 57.8 %copy-start.6 = (f32[96]{0:T(128)S(1)}, f32[96]{0:T(128)}, u32[]{:S(2)}) copy-start(f32[96]{0:T(128)} %param.35) | copy-start | bytes 1156
  83.2 22.3 %copy-start.5 = (bf16[512,128]{1,0:T(8,128)(2,1)S(1)}, bf16[512,128]{1,0:T(8,128)(2,1)}, u32[]{:S(2)}) copy-start(bf16[512,128]{1,0:T(8,128)(2,1)} %param.33) | copy-start | bytes 393220
  84.0 73.4 %all-gather.18.cloned.1.call-start = ((), (), s32[]{:S(2)}) async-start(), calls=%async_computation.6 | async-start | bytes 1310720 | tf_op jit(solution)/shard_map/all_gather | solution.py:188
  103.4 2.1 copy-start.2
  105.2 26.8 %copy-start.8 = (f32[96]{0:T(128)S(1)}, f32[96]{0:T(128)}, u32[]{:S(2)}) copy-start(f32[96]{0:T(128)} %param.34) | copy-start | bytes 1156
  106.7 27.1 %copy-start.10 = (f32[2]{0:T(128)S(1)}, f32[2]{0:T(128)}, u32[]{:S(2)}) copy-start(f32[2]{0:T(128)} %param.36) | copy-start | bytes 28
  106.8 83.2 %all-gather.16.cloned.1.call-start = ((), (), s32[]{:S(2)}) async-start(), calls=%async_computation.5 | async-start | bytes 1966080 | tf_op jit(solution)/shard_map/all_gather | solution.py:187
  132.3 0.7 copy-start.3
  133.1 111.0 %all-gather.20.cloned.1.call-start = ((), (), s32[]{:S(2)}) async-start(), calls=%async_computation.7 | async-start | bytes 4718592 | tf_op jit(solution)/shard_map/all_gather | solution.py:207
  191.5 52.5 %copy-start.1 = (bf16[128,2048]{1,0:T(8,128)(2,1)S(1)}, bf16[128,2048]{1,0:T(8,128)(2,1)}, u32[]{:S(2)}) copy-start(bf16[128,2048]{1,0:T(8,128)(2,1)} %param.20) | copy-start | bytes 1572868
  213.9 30.2 %all-to-all-start = ((bf16[8,128,128]{1,2,0:T(8,128)(2,1)}), bf16[8,128,128]{1,2,0:T(8,128)(2,1)S(1)}, u32[]{:S(2)}, u32[]{:S(2)}) async-start(bf16[8,128,128]{1,2,0:T(8,128)(2,1)} %copy.47), calls=%async_computation | async-start | bytes 524288 | tf_op jit(solution)/shard_map/all_to_all | solution.py:203
Sparse Core Ops, SparseCore 0:
  8.9 32.3 all-gather.7
  43.0 37.5 all-gather.9
  82.3 21.0 all-gather.13
  104.9 24.8 all-gather.11
  131.5 25.8 all-gather.17
  159.1 30.7 all-gather.15
  191.5 52.4 all-gather.19
where the time goes:
time: 256 us; the launch traced here: 255 us
  waiting for transfers between devices  125 us (49%)
  blocking collectives  56.2 us (22%)
  matrix products  33 us (13%)
  other arithmetic  14 us (5%)
  between operations  13.9 us (5%)
  local copies, waits for them, and re-layouts  7.88 us (3%)
  starting transfers between devices  4.82 us (2%)
    all_gather x1, waiting for transfers between devices, shards(): lax.all_gather(down_q, 'tp', axis=0, tiled=True)  33.1 us
    all_gather x1, waiting for transfers between devices, shards(): lax.all_gather(keys, 'sp', axis=0, tiled=True)  29.4 us
    all_gather x1, waiting for transfers between devices, shards(): lax.all_gather(out_weight, 'tp', axis=0, tiled=True)  25.6 us
    all_gather x1, waiting for transfers between devices, shards(): lax.all_gather(query_latent, 'tp', axis=0, tiled=True)  23 us
    all_gather x1, blocking collectives, shards(): modulations = lax.all_gather(summed, 'tp', axis=1, tiled=True)  14.7 us
    all_gather x1, blocking collectives, shards(): lax.all_gather(rope_rows[:own_rows], 'tp', axis=0, tiled=True)  13.1 us
    psum x1, blocking collectives, shards(): summed = lax.psum(partial_value, 'sp')  11.5 us
    dot_general x5, matrix products, absorb_block(): jnp.einsum('qhk,khd->qhd', weights.astype(jnp.bfloat16), value_block, pre...  10.7 us
  transfers between devices with their start and end apart: 8, of which 6 were waited for; matrix products, arithmetic and copies ran while one was open for 20% of the time, Pallas kernels for 0%

commit v1 on v0

--- a/solution.py
+++ b/solution.py
@@ -142,7 +142,8 @@
         axis=0,
     )
     summed = lax.psum(partial_value, "sp")
-    modulations = lax.all_gather(summed, "tp", axis=1, tiled=True)
+    parts = lax.all_gather(summed, "tp")
+    modulations = jnp.concatenate(parts, axis=1)
     normed = modulate(latent, norm_gain, modulations[0], modulations[1])
     context_normed = modulate(context, norm_gain, modulations[3], modulations[4])
     stacked = jnp.concatenate([normed, context_normed], axis=0)

time: 256 us -> 256 us (level)
  no operation moved by 1% of the time
where the time goes in v1:
time: 256 us; the launch traced here: 255 us
  waiting for transfers between devices  125 us (49%)
  blocking collectives  56.2 us (22%)
  matrix products  33 us (13%)
  other arithmetic  14 us (5%)
  between operations  13.9 us (5%)
  local copies, waits for them, and re-layouts  7.88 us (3%)
  starting transfers between devices  4.82 us (2%)
    all_gather x1, waiting for transfers between devices, shards(): lax.all_gather(down_q, 'tp', axis=0, tiled=True)  33.1 us
    all_gather x1, waiting for transfers between devices, shards(): lax.all_gather(keys, 'sp', axis=0, tiled=True)  29.4 us
    all_gather x1, waiting for transfers between devices, shards(): lax.all_gather(out_weight, 'tp', axis=0, tiled=True)  25.6 us
    all_gather x1, waiting for transfers between devices, shards(): lax.all_gather(query_latent, 'tp', axis=0, tiled=True)  23 us
    all_gather x1, blocking collectives, shards(): parts = lax.all_gather(summed, 'tp')  14.7 us
    all_gather x1, blocking collectives, shards(): lax.all_gather(rope_rows[:own_rows], 'tp', axis=0, tiled=True)  13.1 us
    psum x1, blocking collectives, shards(): summed = lax.psum(partial_value, 'sp')  11.5 us
    dot_general x5, matrix products, absorb_block(): jnp.einsum('qhk,khd->qhd', weights.astype(jnp.bfloat16), value_block, pre...  10.7 us
  transfers between devices with their start and end apart: 8, of which 6 were waited for; matrix products, arithmetic and copies ran while one was open for 20% of the time, Pallas kernels for 0%

profile of v1, /device:TPU:0, one launch (start us, length us, event | category | flops | bytes accessed | tf_op | source)
XLA Modules:
  0.0 254.6 jit_solution(13016957012956123958)
XLA Ops:
  9.5 1.3 fusion.62
  13.5 11.5 %psum.7 = f32[1,5,256]{2,1,0:T(8,128)S(1)} all-reduce(f32[1,5,256]{2,1,0:T(8,128)S(1)} %maximum_bitcast_fusion), channel_id=1, replica_groups=mesh['sp'=4,'tp'=8] {'sp'}, use_global_device_ids=true, to_apply=%region_0.1 | all-reduce | flops 1280 | bytes 10240 | tf_op jit(solution)/shard_map/psum | solution.py:144
  25.0 14.7 %all_gather.37 = f32[8,5,256]{2,1,0:T(8,128)S(1)} all-gather(f32[1,5,256]{2,1,0:T(8,128)S(1)} %psum.7), channel_id=1, replica_groups=mesh['sp'=4,'tp'=8] {'tp'}, dimensions={0}, use_global_device_ids=true | all-gather | bytes 46080 | tf_op jit(solution)/shard_map/all_gather | solution.py:145
  44.4 2.2 multiply_reduce_fusion.3
  47.6 33.1 %all-gather.10.cloned.1.call-done = bf16[2048,768]{1,0:T(8,128)(2,1)} async-done(((bf16[256,768]{1,0:T(8,128)(2,1)}), bf16[2048,768]{1,0:T(8,128)(2,1)}) %all-gather.10.cloned.1.call-update) | async-done | bytes 3145744 | tf_op jit(solution)/shard_map/all_gather | solution.py:151
  80.7 2.6 %multiply_reduce_fusion.2 = (f32[128]{0:T(128)S(1)}, f32[128,768]{1,0:T(8,128)S(1)}) fusion(bf16[128,2048]{1,0:T(8,128)(2,1)S(1)} %fusion.28, bf16[2048,768]{1,0:T(8,128)(2,1)} %all-gather.10.cloned.1.call-done), kind=kOutput, calls=%fused_computation.55 | convolution fusion | flops 402849664 | bytes 4063744 | tf_op jit(solution)/shard_map/dot_general | solution.py:155
  84.4 13.1 %all_gather.44 = bf16[1024,32]{0,1:T(8,128)(2,1)S(1)} all-gather(bf16[128,32]{0,1:T(8,128)(2,1)S(1)} %slice.92), channel_id=1, replica_groups=mesh['sp'=4,'tp'=8] {'tp'}, dimensions={0}, use_global_device_ids=true | all-gather | bytes 73728 | tf_op jit(solution)/shard_map/all_gather | solution.py:165
  97.9 5.5 %all-gather.14.cloned.1.call-done = bf16[1024,512]{1,0:T(8,128)(2,1)} async-done(((bf16[128,512]{1,0:T(8,128)(2,1)}), bf16[1024,512]{1,0:T(8,128)(2,1)}) %all-gather.14.cloned.1.call-update) | async-done | bytes 1048592 | tf_op jit(solution)/shard_map/all_gather | solution.py:164
  103.4 1.8 fusion.69
  106.8 23.0 %all-gather.12.cloned.1.call-done = bf16[1024,768]{1,0:T(8,128)(2,1)} async-done(((bf16[128,768]{1,0:T(8,128)(2,1)}), bf16[1024,768]{1,0:T(8,128)(2,1)}) %all-gather.12.cloned.1.call-update) | async-done | bytes 1572880 | tf_op jit(solution)/shard_map/all_gather | solution.py:163
  129.8 2.1 fusion.68
  134.6 8.7 %all_gather.39 = bf16[128,2,96]{2,0,1:T(8,128)(2,1)S(1)} all-gather(bf16[32,2,96]{2,0,1:T(8,128)(2,1)S(1)} %multiply_convert_fusion.2), channel_id=1, replica_groups=mesh['sp'=4,'tp'=8] {'sp'}, dimensions={0}, use_global_device_ids=true | all-gather | bytes 61440 | tf_op jit(solution)/shard_map/all_gather | solution.py:171
  143.3 8.2 %all_gather.42 = bf16[128,2,64]{2,0,1:T(8,128)(2,1)S(1)} all-gather(bf16[32,2,64]{2,0,1:T(8,128)(2,1)S(1)} %copy.43), channel_id=1, replica_groups=mesh['sp'=4,'tp'=8] {'sp'}, dimensions={0}, use_global_device_ids=true | all-gather | bytes 40960 | tf_op jit(solution)/shard_map/all_gather | solution.py:172
  151.6 5.9 %all-gather.18.cloned.1.call-done = bf16[4096,2,64]{0,2,1:T(8,128)(2,1)} async-done(((bf16[1024,2,64]{0,2,1:T(8,128)(2,1)}), bf16[4096,2,64]{0,2,1:T(8,128)(2,1)}) %all-gather.18.cloned.1.call-update) | async-done | bytes 1048592 | tf_op jit(solution)/shard_map/all_gather | solution.py:189
  157.4 2.3 copy.60
  160.5 29.4 %all-gather.16.cloned.1.call-done = bf16[4096,2,96]{0,2,1:T(8,128)(2,1)} async-done(((bf16[1024,2,96]{0,2,1:T(8,128)(2,1)}), bf16[4096,2,96]{0,2,1:T(8,128)(2,1)}) %all-gather.16.cloned.1.call-update) | async-done | bytes 1572880 | tf_op jit(solution)/shard_map/all_gather | solution.py:188
  189.9 1.6 copy.59
  191.5 21.5 %while.14 = (s32[]{:T(128)}, f32[1024,2]{0,1:T(2,128)S(1)}, f32[1024,2]{0,1:T(2,128)S(1)}, f32[1024,2,64]{0,2,1:T(8,128)S(1)}, bf16[4,1024,2,96]{1,3,2,0:T(8,128...) while((s32[]{:T(128)}, f32[1024,2]{0,1:T(2,128)S(1)}, ...), condition=%wide.region_13.14_spmd, body=%wide.region_10.13_spmd.sunk | while | flops 688132096 | bytes 27394648 | solution.py:199
  191.5 1.3 bitcast_reduce_fusion.2
  192.9 1.4 fusion.97
  194.3 2.6 %fusion.98 = f32[1024,2,64]{0,2,1:T(8,128)S(1)} fusion(f32[2,1024,1024]{2,1,0:T(8,128)S(1)} %get-tuple-element.168, f32[1024,2]{0,1:T(2,128)S(1)} %max.4, f32[1024,2,64]{0,2,1:T(8,128)S(1)} %get-tuple-element.182, bf16[4,1024,2,64]{1,3,2,0:T(8,128)(2,1)} %get-tuple-element.193, s32[]{:T(128)} %get-tuple-element.179, f32[1024,2]{0,1:T(2,128)S(1)} %get-tuple-element.170), kind=kOutput, calls=%fused_computation.7.clone.1 | convolution fusion | flops 274989056 | bytes 9716224 | tf_op jit(solution)/shard_map/while/body/eval_jaxpr/qhk,khd->qhd/dot_general | solution.py:97
  196.9 1.3 bitcast_reduce_fusion.2
  198.2 1.4 fusion.97
  199.6 2.6 %fusion.98 = f32[1024,2,64]{0,2,1:T(8,128)S(1)} fusion(f32[2,1024,1024]{2,1,0:T(8,128)S(1)} %get-tuple-element.168, f32[1024,2]{0,1:T(2,128)S(1)} %max.4, f32[1024,2,64]{0,2,1:T(8,128)S(1)} %get-tuple-element.182, bf16[4,1024,2,64]{1,3,2,0:T(8,128)(2,1)} %get-tuple-element.193, s32[]{:T(128)} %get-tuple-element.179, f32[1024,2]{0,1:T(2,128)S(1)} %get-tuple-element.170), kind=kOutput, calls=%fused_computation.7.clone.1 | convolution fusion | flops 274989056 | bytes 9716224 | tf_op jit(solution)/shard_map/while/body/eval_jaxpr/qhk,khd->qhd/dot_general | solution.py:97
  202.3 1.3 bitcast_reduce_fusion.2
  203.6 1.4 fusion.97
  205.0 2.6 %fusion.98 = f32[1024,2,64]{0,2,1:T(8,128)S(1)} fusion(f32[2,1024,1024]{2,1,0:T(8,128)S(1)} %get-tuple-element.168, f32[1024,2]{0,1:T(2,128)S(1)} %max.4, f32[1024,2,64]{0,2,1:T(8,128)S(1)} %get-tuple-element.182, bf16[4,1024,2,64]{1,3,2,0:T(8,128)(2,1)} %get-tuple-element.193, s32[]{:T(128)} %get-tuple-element.179, f32[1024,2]{0,1:T(2,128)S(1)} %get-tuple-element.170), kind=kOutput, calls=%fused_computation.7.clone.1 | convolution fusion | flops 274989056 | bytes 9716224 | tf_op jit(solution)/shard_map/while/body/eval_jaxpr/qhk,khd->qhd/dot_general | solution.py:97
  209.0 1.4 fusion.97
  210.4 2.6 %fusion.98 = f32[1024,2,64]{0,2,1:T(8,128)S(1)} fusion(f32[2,1024,1024]{2,1,0:T(8,128)S(1)} %get-tuple-element.168, f32[1024,2]{0,1:T(2,128)S(1)} %max.4, f32[1024,2,64]{0,2,1:T(8,128)S(1)} %get-tuple-element.182, bf16[4,1024,2,64]{1,3,2,0:T(8,128)(2,1)} %get-tuple-element.193, s32[]{:T(128)} %get-tuple-element.179, f32[1024,2]{0,1:T(2,128)S(1)} %get-tuple-element.170), kind=kOutput, calls=%fused_computation.7.clone.1 | convolution fusion | flops 274989056 | bytes 9716224 | tf_op jit(solution)/shard_map/while/body/eval_jaxpr/qhk,khd->qhd/dot_general | solution.py:97
  213.9 4.6 %all-to-all-start = ((bf16[8,128,128]{1,2,0:T(8,128)(2,1)}), bf16[8,128,128]{1,2,0:T(8,128)(2,1)S(1)}, u32[]{:S(2)}, u32[]{:S(2)}) async-start(bf16[8,128,128]{1,2,0:T(8,128)(2,1)} %copy.47), calls=%async_computation | async-start | bytes 524288 | tf_op jit(solution)/shard_map/all_to_all | solution.py:204
  218.5 25.6 %all-gather.20.cloned.1.call-done = bf16[1024,2048]{1,0:T(8,128)(2,1)} async-done(((bf16[128,2048]{1,0:T(8,128)(2,1)}), bf16[1024,2048]{1,0:T(8,128)(2,1)}) %all-gather.20.cloned.1.call-update) | async-done | bytes 4194320 | tf_op jit(solution)/shard_map/all_gather | solution.py:208
  244.1 3.7 %fusion.20 = bf16[128,2048]{1,0:T(8,128)(2,1)} fusion(bf16[128,1024]{0,1:T(8,128)(2,1)S(1)} %bitcast.115, bf16[1024,2048]{1,0:T(8,128)(2,1)} %all-gather.20.cloned.1.call-done, bf16[128,2048]{1,0:T(8,128)(2,1)S(1)} %copy-done.1, f32[2048]{0:T(1024)S(1)} %bitcast.117), kind=kOutput, calls=%fused_computation.20 | convolution fusion | flops 537919488 | bytes 5513216 | tf_op jit(solution)/shard_map/dot_general | solution.py:206
  (113 shorter events, 19.9 us)
Async XLA Ops:
  6.5 123.3 %copy-start = (bf16[768,192]{0,1:T(8,128)(2,1)S(1)}, bf16[768,192]{0,1:T(8,128)(2,1)}, u32[]{:S(2)}) copy-start(bf16[768,192]{0,1:T(8,128)(2,1)} %param.31) | copy-start | bytes 884740
  6.5 37.9 %all-gather.8.cloned.1.call-start = ((), (), s32[]{:S(2)}) async-start(), calls=%async_computation.1 | async-start | bytes 2359296 | tf_op jit(solution)/shard_map/all_gather | solution.py:152
  7.3 40.3 %copy-start.7 = (bf16[768]{0:T(1024)(128)(2,1)S(1)}, bf16[768]{0:T(1024)(128)(2,1)}, u32[]{:S(2)}) copy-start(bf16[768]{0:T(1024)(128)(2,1)} %param.29) | copy-start | bytes 4612
  7.3 73.4 %all-gather.10.cloned.1.call-start = ((), (), s32[]{:S(2)}) async-start(), calls=%async_computation.2 | async-start | bytes 3538944 | tf_op jit(solution)/shard_map/all_gather | solution.py:151
  8.0 95.4 %all-gather.14.cloned.1.call-start = ((), (), s32[]{:S(2)}) async-start(), calls=%async_computation.4 | async-start | bytes 1179648 | tf_op jit(solution)/shard_map/all_gather | solution.py:164
  44.4 39.7 %copy-start.9 = (bf16[2048,32]{0,1:T(8,128)(2,1)S(1)}, bf16[2048,32]{0,1:T(8,128)(2,1)}, u32[]{:S(2)}) copy-start(bf16[2048,32]{0,1:T(8,128)(2,1)} %param.28) | copy-start | bytes 393220
  46.7 56.7 %copy-start.4 = (bf16[512,128]{1,0:T(8,128)(2,1)S(1)}, bf16[512,128]{1,0:T(8,128)(2,1)}, u32[]{:S(2)}) copy-start(bf16[512,128]{1,0:T(8,128)(2,1)} %param.32) | copy-start | bytes 393220
  47.5 82.3 %all-gather.12.cloned.1.call-start = ((), (), s32[]{:S(2)}) async-start(), calls=%async_computation.3 | async-start | bytes 1769472 | tf_op jit(solution)/shard_map/all_gather | solution.py:163
  47.5 57.8 %copy-start.6 = (f32[96]{0:T(128)S(1)}, f32[96]{0:T(128)}, u32[]{:S(2)}) copy-start(f32[96]{0:T(128)} %param.35) | copy-start | bytes 1156
  83.2 22.3 %copy-start.5 = (bf16[512,128]{1,0:T(8,128)(2,1)S(1)}, bf16[512,128]{1,0:T(8,128)(2,1)}, u32[]{:S(2)}) copy-start(bf16[512,128]{1,0:T(8,128)(2,1)} %param.33) | copy-start | bytes 393220
  84.0 73.4 %all-gather.18.cloned.1.call-start = ((), (), s32[]{:S(2)}) async-start(), calls=%async_computation.6 | async-start | bytes 1310720 | tf_op jit(solution)/shard_map/all_gather | solution.py:189
  103.4 2.1 copy-start.2
  105.2 26.8 %copy-start.8 = (f32[96]{0:T(128)S(1)}, f32[96]{0:T(128)}, u32[]{:S(2)}) copy-start(f32[96]{0:T(128)} %param.34) | copy-start | bytes 1156
  106.7 27.2 %copy-start.10 = (f32[2]{0:T(128)S(1)}, f32[2]{0:T(128)}, u32[]{:S(2)}) copy-start(f32[2]{0:T(128)} %param.36) | copy-start | bytes 28
  106.8 83.2 %all-gather.16.cloned.1.call-start = ((), (), s32[]{:S(2)}) async-start(), calls=%async_computation.5 | async-start | bytes 1966080 | tf_op jit(solution)/shard_map/all_gather | solution.py:188
  132.3 0.7 copy-start.3
  133.1 111.0 %all-gather.20.cloned.1.call-start = ((), (), s32[]{:S(2)}) async-start(), calls=%async_computation.7 | async-start | bytes 4718592 | tf_op jit(solution)/shard_map/all_gather | solution.py:208
  191.5 52.5 %copy-start.1 = (bf16[128,2048]{1,0:T(8,128)(2,1)S(1)}, bf16[128,2048]{1,0:T(8,128)(2,1)}, u32[]{:S(2)}) copy-start(bf16[128,2048]{1,0:T(8,128)(2,1)} %param.20) | copy-start | bytes 1572868
  213.9 30.2 %all-to-all-start = ((bf16[8,128,128]{1,2,0:T(8,128)(2,1)}), bf16[8,128,128]{1,2,0:T(8,128)(2,1)S(1)}, u32[]{:S(2)}, u32[]{:S(2)}) async-start(bf16[8,128,128]{1,2,0:T(8,128)(2,1)} %copy.47), calls=%async_computation | async-start | bytes 524288 | tf_op jit(solution)/shard_map/all_to_all | solution.py:204
Sparse Core Ops, SparseCore 0:
  8.9 32.3 all-gather.7
  43.0 37.5 all-gather.9
  82.3 21.0 all-gather.13
  104.9 24.8 all-gather.11
  131.5 25.8 all-gather.17
  159.1 30.7 all-gather.15
  191.5 52.4 all-gather.19
